TPU v7x, 32 devices: a whole 2x2x4 slice. The times are simulated.
32 devices in a mesh: sp: 4 (over z), fs: 4 (over y, core), tp: 2 (over x).
Axes of the slice: x: 2, y: 2, z: 4, core: 2. Of those that a mesh axis runs over, the one named last changes fastest.
Arguments:
- tokens: bfloat16 [8, 2048, 2048], P('fs', ('sp', 'tp')), may hold values from -6 to 6
- norm_gain: float32 [2048], replicated, may hold values from 0.1 to 1.9
- w_pool_in: bfloat16 [2048, 1024], P('fs', 'tp'), may hold values from -0.125 to 0.125
- pool_mix: bfloat16 [8, 128, 128], replicated, may hold values from -0.5 to 0.5
- pool_scale: float32 [1024], replicated, may hold values from 0.1 to 1.9
- w_query: bfloat16 [2048, 1024], P('fs', 'tp'), may hold values from -0.13258252 to 0.13258252
- w_key: bfloat16 [2048, 1024], P('fs', 'tp'), may hold values from -0.508233 to 0.508233
- w_value: bfloat16 [2048, 1024], P('fs', 'tp'), may hold values from -0.125 to 0.125
- gate_cache: float32 [8, 8, 2048], P('fs', 'tp'), may hold values from -258 to 0, as said below
- w_out_pool: bfloat16 [1024, 2048], P('tp', 'fs'), may hold values from -0.125 to 0.125
- w_out_attn: bfloat16 [1024, 2048], P('tp', 'fs'), may hold values from -0.75 to 0.75
Outputs:
- mixed: bfloat16 [8, 2048, 2048], P('fs', ('sp', 'tp'))
Inputs may be any that keep to these rules, and one draw needn't show every extreme that they name: `gate_cache`: each head's values never rise along the positions.
All inputs are finite; a program needn't handle non-finite values.
Results may differ from a plain program's by a relative error of at most 0.014.
Values may be sent and summed in bfloat16 or wider, within the bound.
A program may use at most 128 MiB of HBM per device.

v0:
```python
import jax
import jax.numpy as jnp
from jax import lax
from jax.sharding import PartitionSpec as P

HEAD_DIM = 128
GROUP_WIDTH = 128
norm_eps = 1e-06
widest = 16
masked_score = -1e30


def shifted(x, axis, by):
    length = lax.axis_size(axis)
    pairs = [(i, i + by) for i in range(length) if 0 <= i + by < length]
    return lax.ppermute(x, axis, pairs)


def window_sums(extended):
    outcome = []
    current = extended
    offset = 1
    for doubling in range(4):
        padding = jnp.zeros((offset, extended.shape[1]), jnp.float32)
        current = current + jnp.concatenate([padding, current[:-offset]], axis=0)
        offset = offset * 2
        outcome.append(current[widest - 1 :])
    return outcome


def pool_branch(projected, border, first_group, first_position, mixing, scaling):
    row_count = projected.shape[0]
    channels = projected.shape[1]
    widened = projected.astype(jnp.float32)
    totals = window_sums(jnp.concatenate([border.astype(jnp.float32), widened], axis=0))
    token_positions = first_position + jnp.arange(row_count)
    window_index = (first_group + jnp.arange(channels) // GROUP_WIDTH) % 4
    averaged = jnp.zeros((row_count, channels), jnp.float32)
    for doubling in range(4):
        counted = jnp.minimum(token_positions + 1, 2 ** (doubling + 1)).astype(jnp.float32)
        picked = (window_index == doubling).astype(jnp.float32)
        averaged = averaged + picked[None, :] * totals[doubling] / counted[:, None]
    departure = (averaged - widened).astype(jnp.bfloat16)
    group_count = channels // GROUP_WIDTH
    mixed_rows = jnp.einsum(
        "tgc,gcd->tgd",
        departure.reshape(row_count, group_count, GROUP_WIDTH),
        mixing,
        preferred_element_type=jnp.float32,
    )
    return (mixed_rows.reshape(row_count, channels) * scaling[None, :]).astype(jnp.bfloat16)


def on_device(
    tokens,
    norm_gain,
    w_pool_in,
    pool_mix,
    pool_scale,
    w_query,
    w_key,
    w_value,
    gate_cache,
    w_out_pool,
    w_out_attn,
):
    tp_index = lax.axis_index("tp")
    tp_count = lax.axis_size("tp")
    seq_count = tokens.shape[0]
    own_count = tokens.shape[1]
    token_count = own_count * tp_count
    first_position = lax.axis_index("sp") * token_count
    own_rows = tokens.astype(jnp.float32)
    normed = (
        own_rows
        * lax.rsqrt(jnp.mean(own_rows * own_rows, axis=-1, keepdims=True) + norm_eps)
        * norm_gain[None, None, :]
    ).astype(jnp.bfloat16)
    pool_full, query_full, key_full, value_full, out_pool_full, out_attn_full = (
        lax.all_gather(w_pool_in, "fs", axis=0, tiled=True),
        lax.all_gather(w_query, "fs", axis=0, tiled=True),
        lax.all_gather(w_key, "fs", axis=0, tiled=True),
        lax.all_gather(w_value, "fs", axis=0, tiled=True),
        lax.all_gather(w_out_pool, "fs", axis=1, tiled=True),
        lax.all_gather(w_out_attn, "fs", axis=1, tiled=True),
    )
    pool_cols = w_pool_in.shape[1]
    attn_cols = w_query.shape[1]
    shard_rows = lax.all_gather(normed, "tp", axis=1, tiled=True)
    projected = jnp.concatenate(
        [
            jnp.dot(shard_rows, pool_full, preferred_element_type=jnp.float32).astype(jnp.bfloat16),
            jnp.dot(shard_rows, query_full, preferred_element_type=jnp.float32).astype(
                jnp.bfloat16
            ),
            jnp.dot(shard_rows, key_full, preferred_element_type=jnp.float32).astype(jnp.bfloat16),
            jnp.dot(shard_rows, value_full, preferred_element_type=jnp.float32).astype(
                jnp.bfloat16
            ),
        ],
        axis=2,
    )
    pool_in = projected[:, :, :pool_cols]
    query_proj = projected[:, :, pool_cols : pool_cols + attn_cols]
    key_proj = projected[:, :, pool_cols + attn_cols : pool_cols + 2 * attn_cols]
    value_proj = projected[:, :, pool_cols + 2 * attn_cols :]
    group_local = pool_cols // GROUP_WIDTH
    mixing = lax.dynamic_slice_in_dim(pool_mix, tp_index * group_local, group_local, 0)
    scaling = lax.dynamic_slice_in_dim(pool_scale, tp_index * pool_cols, pool_cols, 0)
    borders = shifted(pool_in[:, token_count - (widest - 1) :], "sp", 1)
    pool_out = jnp.stack(
        [
            pool_branch(
                pool_in[member],
                borders[member],
                tp_index * group_local,
                first_position,
                mixing,
                scaling,
            )
            for member in range(seq_count)
        ],
        axis=0,
    )
    head_count = attn_cols // HEAD_DIM
    query_heads = query_proj.reshape(seq_count, token_count, head_count, HEAD_DIM)
    query_gates = jnp.transpose(
        lax.dynamic_slice_in_dim(gate_cache, first_position, token_count, 2), (0, 2, 1)
    )
    query_positions = first_position + jnp.arange(token_count)
    last_position = first_position + token_count - 1
    score_scale = HEAD_DIM ** (-0.5)
    start_state = (
        jnp.full((seq_count, token_count, head_count), masked_score, jnp.float32),
        jnp.zeros((seq_count, token_count, head_count), jnp.float32),
        jnp.zeros((seq_count, token_count, head_count, HEAD_DIM), jnp.float32),
    )
    key_shard = lax.all_gather(key_proj, "sp", axis=1, tiled=True)
    value_shard = lax.all_gather(value_proj, "sp", axis=1, tiled=True)
    key_total = key_shard.shape[1]
    block_rows = 512

    def one_block(block_state, block_index):
        key_start = block_index * block_rows

        def compute(inner_state):
            running_top, running_sum, running_out = inner_state
            key_block = lax.dynamic_slice_in_dim(key_shard, block_index * block_rows, block_rows, 1)
            value_block = lax.dynamic_slice_in_dim(
                value_shard, block_index * block_rows, block_rows, 1
            )
            key_block = key_block.reshape(seq_count, block_rows, head_count, HEAD_DIM)
            value_block = value_block.reshape(seq_count, block_rows, head_count, HEAD_DIM)
            key_gates = lax.dynamic_slice_in_dim(gate_cache, key_start, block_rows, 2)
            scores = (
                jnp.einsum(
                    "sqhd,skhd->sqhk", query_heads, key_block, preferred_element_type=jnp.float32
                )
                * score_scale
            )
            scores = scores + query_gates[:, :, :, None] - key_gates[:, None, :, :]
            allowed = ((key_start + jnp.arange(block_rows))[None, :] <= query_positions[:, None])[
                None, :, None, :
            ]
            scores = jnp.where(allowed, scores, masked_score)
            new_top = jnp.maximum(running_top, jnp.max(scores, axis=3))
            weights = jnp.where(allowed, jnp.exp(scores - new_top[:, :, :, None]), 0.0)
            shrink = jnp.exp(running_top - new_top)
            running_sum = running_sum * shrink + jnp.sum(weights, axis=3)
            running_out = running_out * shrink[:, :, :, None] + jnp.einsum(
                "sqhk,skhd->sqhd",
                weights.astype(jnp.bfloat16),
                value_block,
                preferred_element_type=jnp.float32,
            )
            return (new_top, running_sum, running_out)

        def unchanged(inner_state):
            return inner_state

        return (lax.cond(key_start <= last_position, compute, unchanged, block_state), None)

    result, unused = lax.scan(one_block, start_state, jnp.arange(key_total // block_rows))
    final_top, final_sum, final_out = result
    attn_out = (
        (final_out / final_sum[:, :, :, None])
        .astype(jnp.bfloat16)
        .reshape(seq_count, token_count, attn_cols)
    )
    pool_flat = jnp.transpose(
        pool_out.reshape(seq_count, tp_count, own_count, pool_cols), (1, 0, 2, 3)
    ).reshape(tp_count * seq_count * own_count, pool_cols)
    attn_flat = jnp.transpose(
        attn_out.reshape(seq_count, tp_count, own_count, attn_cols), (1, 0, 2, 3)
    ).reshape(tp_count * seq_count * own_count, attn_cols)
    summed = lax.psum_scatter(
        (
            jnp.dot(pool_flat, out_pool_full, preferred_element_type=jnp.float32)
            + jnp.dot(attn_flat, out_attn_full, preferred_element_type=jnp.float32)
        ).astype(jnp.bfloat16),
        "tp",
        scatter_dimension=0,
        tiled=True,
    ).astype(jnp.float32)
    return summed.astype(jnp.bfloat16).reshape(seq_count, own_count, summed.shape[1])


def solution(mesh):
    placed = (
        P("fs", ("sp", "tp"), None),
        P(),
        P("fs", "tp"),
        P(),
        P(),
        P("fs", "tp"),
        P("fs", "tp"),
        P("fs", "tp"),
        P("fs", "tp", None),
        P("tp", "fs"),
        P("tp", "fs"),
    )
    return jax.shard_map(
        on_device,
        mesh=mesh,
        in_specs=placed,
        out_specs=P("fs", ("sp", "tp"), None),
        check_vma=False,
    )
```

profile of v0, /device:TPU:0, one launch (start us, length us, event | category | flops | bytes accessed | tf_op | source)
XLA Modules:
  0.0 483.2 jit_solution(8892311270368384525)
XLA Ops:
  6.5 0.7 all-gather.16.cloned.1.call-update
  7.3 2.1 fusion.15
  9.4 1.9 fusion.17
  11.4 0.7 all-gather.22.cloned.1.call-update
  12.1 0.5 all-gather.12.cloned.1.call-update
  12.7 1.0 copy.37
  13.8 0.5 all-gather.14.cloned.1.call-update
  14.4 19.8 %all-gather.16.cloned.1.call-done = bf16[2048,512]{1,0:T(8,128)(2,1)} async-done(((bf16[512,512]{1,0:T(8,128)(2,1)}), bf16[2048,512]{1,0:T(8,128)(2,1)}) %all-gather.16.cloned.1.call-update) | async-done | bytes 2097168 | tf_op jit(solution)/shard_map/all_gather | solution.py:82
  34.2 58.3 %all-gather.10.cloned.1.call-done = bf16[2,512,2048]{2,1,0:T(8,128)(2,1)} async-done(((bf16[2,256,2048]{2,1,0:T(8,128)(2,1)}), bf16[2,512,2048]{2,1,0:T(8,128)(2,1)}) %all-gather.10.cloned.1.call-update) | async-done | bytes 4194320 | tf_op jit(solution)/shard_map/all_gather | solution.py:89
  92.5 6.2 %fusion.29 = bf16[2,512,512]{2,1,0:T(8,128)(2,1)} fusion(bf16[2,512,2048]{2,1,0:T(8,128)(2,1)} %all-gather.10.cloned.1.call-done, bf16[2048,512]{1,0:T(8,128)(2,1)} %all-gather.16.cloned.1.call-done), kind=kOutput, calls=%fused_computation.42 | convolution fusion | flops 2148007936 | bytes 7340032 | tf_op jit(solution)/shard_map/dot_general | solution.py:96
  98.8 17.9 %all-gather.22.cloned.1.call-done = bf16[2048,512]{1,0:T(8,128)(2,1)} async-done(((bf16[512,512]{1,0:T(8,128)(2,1)}), bf16[2048,512]{1,0:T(8,128)(2,1)}) %all-gather.22.cloned.1.call-update) | async-done | bytes 2097168 | tf_op jit(solution)/shard_map/all_gather | solution.py:83
  116.7 6.2 %fusion.35 = bf16[2,512,512]{2,1,0:T(8,128)(2,1)} fusion(bf16[2,512,2048]{2,1,0:T(8,128)(2,1)} %all-gather.10.cloned.1.call-done, bf16[2048,512]{1,0:T(8,128)(2,1)} %all-gather.22.cloned.1.call-done), kind=kOutput, calls=%fused_computation.44 | convolution fusion | flops 2148007936 | bytes 7340032 | tf_op jit(solution)/shard_map/dot_general | solution.py:97
  122.9 0.7 all-gather.26.cloned.1.call-update
  123.7 0.7 dynamic_slice.23
  124.4 16.3 %all-gather.12.cloned.1.call-done = bf16[2048,512]{1,0:T(8,128)(2,1)} async-done(((bf16[512,512]{1,0:T(8,128)(2,1)}), bf16[2048,512]{1,0:T(8,128)(2,1)}) %all-gather.12.cloned.1.call-update) | async-done | bytes 2097168 | tf_op jit(solution)/shard_map/all_gather | solution.py:80
  140.7 5.2 %fusion.26 = bf16[2,512,512]{2,1,0:T(8,128)(2,1)S(1)} fusion(bf16[2,512,2048]{2,1,0:T(8,128)(2,1)} %all-gather.10.cloned.1.call-done, bf16[2048,512]{1,0:T(8,128)(2,1)} %all-gather.12.cloned.1.call-done), kind=kOutput, calls=%fused_computation.41 | convolution fusion | flops 2148007936 | bytes 7340032 | tf_op jit(solution)/shard_map/dot_general | solution.py:92
  145.9 4.0 collective-permute-start
  149.9 14.8 %all-gather.20.cloned.1.call-done = bf16[2048,512]{0,1:T(8,128)(2,1)} async-done(((bf16[512,512]{0,1:T(8,128)(2,1)}), bf16[2048,512]{0,1:T(8,128)(2,1)}) %all-gather.20.cloned.1.call-update) | async-done | bytes 2097168 | tf_op jit(solution)/shard_map/all_gather | solution.py:81
  164.7 6.2 %fusion.32 = bf16[2,512,512]{1,2,0:T(8,128)(2,1)} fusion(bf16[2,512,2048]{2,1,0:T(8,128)(2,1)} %all-gather.10.cloned.1.call-done, bf16[2048,512]{0,1:T(8,128)(2,1)} %all-gather.20.cloned.1.call-done), kind=kOutput, calls=%fused_computation.43 | convolution fusion | flops 2148007936 | bytes 7340032 | tf_op jit(solution)/shard_map/dot_general | solution.py:93
  171.2 2.3 copy.39
  173.5 0.8 fusion.71
  174.6 0.5 fusion.38
  176.3 2.9 fusion.67
  179.6 0.7 reshape.190
  180.2 0.8 copy.34
  181.1 1.4 convolution_bitcast_fusion
  182.5 0.7 reshape.192
  183.2 0.8 copy.36
  184.4 4.3 all-gather.14.cloned.1.call-done
  188.7 7.2 %fusion.79 = f32[1024,2048]{1,0:T(8,128)} fusion(bf16[1024,512]{1,0:T(8,128)(2,1)S(1)} %bitcast.129, bf16[512,2048]{1,0:T(8,128)(2,1)} %all-gather.14.cloned.1.call-done), kind=kOutput, calls=%fused_computation.123 | convolution fusion | flops 2147483648 | bytes 11534336 | tf_op jit(solution)/shard_map/dot_general | solution.py:198
  195.9 75.1 %all-gather.18.cloned.1.call-done = bf16[2,2048,512]{2,1,0:T(8,128)(2,1)} async-done(((bf16[2,512,512]{2,1,0:T(8,128)(2,1)}), bf16[2,2048,512]{2,1,0:T(8,128)(2,1)}) %all-gather.18.cloned.1.call-update) | async-done | bytes 4194320 | tf_op jit(solution)/shard_map/all_gather | solution.py:138
  271.0 6.3 %copy.38 = bf16[2,2048,512]{1,2,0:T(8,128)(2,1)} copy(bf16[2,2048,512]{2,1,0:T(8,128)(2,1)} %all-gather.18.cloned.1.call-done) | data formatting | bytes 8388608
  277.3 74.5 %all-gather.24.cloned.1.call-done = bf16[2,2048,512]{2,1,0:T(8,128)(2,1)} async-done(((bf16[2,512,512]{2,1,0:T(8,128)(2,1)}), bf16[2,2048,512]{2,1,0:T(8,128)(2,1)}) %all-gather.24.cloned.1.call-update) | async-done | bytes 4194320 | tf_op jit(solution)/shard_map/all_gather | solution.py:139
  351.9 6.3 %copy.40 = bf16[2,2048,512]{1,2,0:T(8,128)(2,1)} copy(bf16[2,2048,512]{2,1,0:T(8,128)(2,1)} %all-gather.24.cloned.1.call-done) | data formatting | bytes 8388608
  358.4 1.0 copy-done.3
  359.5 17.2 %while.15 = (s32[]{:T(128)}, f32[2,512,4]{1,2,0:T(4,128)S(1)}, f32[2,512,4]{1,2,0:T(4,128)S(1)}, f32[2,512,4,128]{1,3,2,0:T(8,128)S(1)}, s32[4]{0:T(128)S(1)}, /...) while((s32[]{:T(128)}, f32[2,512,4]{1,2,0:T(4,128)S(1)}, ...), condition=%wide.region_6.7_spmd.clone, body=%wide.region_1.6_spmd.clone.sunk | while | flops 1114907648 | bytes 38154664 | solution.py:183
  359.5 0.6 dynamic_slice.35
  360.7 12.1 %conditional.3 = ((f32[2,512,4]{1,2,0:T(4,128)S(1)}, f32[2,512,4]{1,2,0:T(4,128)S(1)}, f32[2,512,4,128]{1,3,2,0:T(8,128)S(1)})) conditional(s32[]{:T(128)} %convert_element_type.217, (f32[2,512,4]{1,2,0:T(4,128)S(1)}, f32[2,512,4]{1,2,0:T(4,128)S(1)}, f32[2,512,4,128]{1,3,2,0:T(8,128)S(1)}) %tuple.49, (s32[]{:T(128)}, s32[]{:T(128)}, s32[]{:T(128)}, ...), branch_computations={%region_2.2_spmd, %region_3.5_spmd} | conditional | flops 1114907648 | bytes 38152320 | solution.py:181
  361.7 1.7 constant_dynamic-slice_fusion
  363.4 2.6 fusion.6
  366.0 3.2 fusion.5
  369.2 3.5 bitcast_add_fusion.1
  372.8 0.6 dynamic_slice.35
  374.1 0.6 dynamic_slice.35
  375.4 0.6 dynamic_slice.35
  377.3 1.5 copy.46
  378.8 8.4 %add_convert_fusion = bf16[1024,2048]{1,0:T(8,128)(2,1)} fusion(f32[1024,2048]{1,0:T(8,128)} %fusion.79, bf16[1024,512]{1,0:T(8,128)(2,1)S(1)} %bitcast.130, bf16[512,2048]{1,0:T(8,128)(2,1)} %all-gather.26.cloned.1.call-done), kind=kOutput, calls=%fused_computation.22 | convolution fusion | flops 2151677952 | bytes 15728640 | tf_op jit(solution)/shard_map/dot_general | solution.py:199
  387.2 89.2 %reduce-scatter.2.cloned.1.call-done = bf16[512,2048]{1,0:T(8,128)(2,1)} async-done(((bf16[1024,2048]{1,0:T(8,128)(2,1)}), bf16[512,2048]{1,0:T(8,128)(2,1)}) %reduce-scatter.2.cloned.1.call-update) | async-done | bytes 2097168 | tf_op jit(solution)/shard_map/reduce_scatter | solution.py:196
  (72 shorter events, 4.1 us)
Async XLA Ops:
  6.5 172.7 %copy-start = (bf16[8,128,128]{2,1,0:T(8,128)(2,1)S(1)}, bf16[8,128,128]{2,1,0:T(8,128)(2,1)}, u32[]{:S(2)}) copy-start(bf16[8,128,128]{2,1,0:T(8,128)(2,1)} %param.18) | copy-start | bytes 786436
  6.5 2.9 copy-start.2
  6.5 2.9 copy-start.6
  6.5 27.7 %all-gather.16.cloned.1.call-start = ((), (), s32[]{:S(2)}) async-start(), calls=%async_computation.4 | async-start | bytes 2621440 | tf_op jit(solution)/shard_map/all_gather | solution.py:82
  7.3 85.2 %all-gather.10.cloned.1.call-start = ((), (), s32[]{:S(2)}) async-start(), calls=%async_computation.1 | async-start | bytes 6291456 | tf_op jit(solution)/shard_map/all_gather | solution.py:89
  11.3 1.4 copy-start.4
  11.3 105.4 %all-gather.22.cloned.1.call-start = ((), (), s32[]{:S(2)}) async-start(), calls=%async_computation.7 | async-start | bytes 2621440 | tf_op jit(solution)/shard_map/all_gather | solution.py:83
  12.0 128.6 %all-gather.12.cloned.1.call-start = ((), (), s32[]{:S(2)}) async-start(), calls=%async_computation.2 | async-start | bytes 2621440 | tf_op jit(solution)/shard_map/all_gather | solution.py:80
  12.6 152.1 %all-gather.20.cloned.1.call-start = ((), (), s32[]{:S(2)}) async-start(), calls=%async_computation.6 | async-start | bytes 2621440 | tf_op jit(solution)/shard_map/all_gather | solution.py:81
  13.7 175.0 %all-gather.14.cloned.1.call-start = ((), (), s32[]{:S(2)}) async-start(), calls=%async_computation.3 | async-start | bytes 2621440 | tf_op jit(solution)/shard_map/all_gather | solution.py:84
  14.3 256.7 %all-gather.18.cloned.1.call-start = ((), (), s32[]{:S(2)}) async-start(), calls=%async_computation.5 | async-start | bytes 5242880 | tf_op jit(solution)/shard_map/all_gather | solution.py:138
  98.7 25.0 %copy-start.8 = (f32[1024]{0:T(1024)S(1)}, f32[1024]{0:T(1024)}, u32[]{:S(2)}) copy-start(f32[1024]{0:T(1024)} %param.19) | copy-start | bytes 12292
  98.7 25.7 %copy-start.5 = (f32[2,4,2048]{2,1,0:T(4,128)S(1)}, f32[2,4,2048]{2,1,0:T(4,128)}, u32[]{:S(2)}) copy-start(f32[2,4,2048]{2,1,0:T(4,128)} %param.23) | copy-start | bytes 196612
  98.7 253.1 %all-gather.24.cloned.1.call-start = ((), (), s32[]{:S(2)}) async-start(), calls=%async_computation.8 | async-start | bytes 5242880 | tf_op jit(solution)/shard_map/all_gather | solution.py:139
  122.9 255.9 %all-gather.26.cloned.1.call-start = ((), (), s32[]{:S(2)}) async-start(), calls=%async_computation.9 | async-start | bytes 2621440 | tf_op jit(solution)/shard_map/all_gather | solution.py:85
  123.6 352.8 %reduce-scatter.2.cloned.1.call-start = ((), (), s32[]{:S(2)}) async-start(), calls=%async_computation.10 | async-start | bytes 6291456 | tf_op jit(solution)/shard_map/reduce_scatter | solution.py:196
  145.9 27.6 %collective-permute-start = (bf16[2,15,512]{2,1,0:T(8,128)(2,1)S(1)}, bf16[2,15,512]{2,1,0:T(8,128)(2,1)}, u32[]{:S(2)}, u32[]{:S(2)}) collective-permute-start(bf16[2,15,512]{2,1,0:T(8,128)(2,1)S(1)} %slice.84), channel_id=1, source_target_pairs={{0,8},{8,16},{16,24},{1,9},{9,17},{17,25},{2,10},{10,18},{18,26},{... | collective-permute-start | bytes 92168 | tf_op jit(solution)/shard_map/ppermute | solution.py:16
  182.5 1.5 copy-start.7
  358.2 1.3 copy-start.3
  387.2 89.2 %copy-start.1 = (bf16[8,128,128]{2,1,0:T(8,128)(2,1)S(1)}, bf16[8,128,128]{2,1,0:T(8,128)(2,1)}, u32[]{:S(2)}) copy-start(bf16[8,128,128]{2,1,0:T(8,128)(2,1)} %param.18) | copy-start | bytes 786436
Sparse Core Ops, SparseCore 0:
  8.9 25.2 all-gather.15
  35.8 56.7 all-gather.9
  94.1 22.5 all-gather.21
  118.1 22.5 all-gather.11
  142.1 22.5 all-gather.19
  166.1 22.5 all-gather.13
  190.3 80.7 all-gather.17
  272.6 79.2 all-gather.23
  353.4 21.0 all-gather.25
  387.3 89.0 reduce-scatter.1
where the time goes:
time: 484 us; the launch traced here: 483 us
  waiting for transfers between devices  374 us (77%)
  matrix products  47.3 us (10%)
  local copies, waits for them, and re-layouts  27 us (6%)
  other arithmetic  13.8 us (3%)
  between operations  13.8 us (3%)
    reduce_scatter x1, waiting for transfers between devices, on_device(): lax.psum_scatter((jnp.dot(pool_flat, out_pool_full, preferred_element_typ...  89.2 us
    all_gather x1, waiting for transfers between devices, on_device(): key_shard = lax.all_gather(key_proj, 'sp', axis=1, tiled=True)  75.1 us
    all_gather x1, waiting for transfers between devices, on_device(): value_shard = lax.all_gather(value_proj, 'sp', axis=1, tiled=True)  74.5 us
    all_gather x1, waiting for transfers between devices, on_device(): shard_rows = lax.all_gather(normed, 'tp', axis=1, tiled=True)  58.3 us
    all_gather x1, waiting for transfers between devices, on_device(): lax.all_gather(w_key, 'fs', axis=0, tiled=True)  19.8 us
    all_gather x1, waiting for transfers between devices, on_device(): lax.all_gather(w_value, 'fs', axis=0, tiled=True)  17.9 us
    unnamed x22, local copies, waits for them, and re-layouts  17 us
    all_gather x1, waiting for transfers between devices, on_device(): lax.all_gather(w_pool_in, 'fs', axis=0, tiled=True)  16.3 us
  transfers between devices with their start and end apart: 11, of which 9 were waited for; matrix products, arithmetic and copies ran while one was open for 16% of the time, Pallas kernels for 0%

commit v1 on v0

--- a/solution.py
+++ b/solution.py
@@ -135,7 +135,14 @@
         jnp.zeros((seq_count, token_count, head_count), jnp.float32),
         jnp.zeros((seq_count, token_count, head_count, HEAD_DIM), jnp.float32),
     )
-    key_shard = lax.all_gather(key_proj, "sp", axis=1, tiled=True)
+    count = lax.axis_size("sp")
+    hops = [(i_2, (i_2 + 1) % count) for i_2 in range(count)]
+    pieces = [key_proj]
+    for far in range(1, count):
+        pieces = [lax.ppermute(pieces[0], "sp", hops), *pieces]
+    out = jnp.concatenate(pieces, axis=1)
+    shift = (lax.axis_index("sp") + 1) * pieces[-1].shape[1]
+    key_shard = jnp.roll(out, shift, axis=1)
     value_shard = lax.all_gather(value_proj, "sp", axis=1, tiled=True)
     key_total = key_shard.shape[1]
     block_rows = 512

time: 484 us -> 427 us (0.88)
  waiting for transfers between devices: 374 us -> 298 us
  local copies, waits for them, and re-layouts: 27 us -> 40.8 us
  starting transfers between devices: 4.34 us -> 9.66 us
    all_gather x1 -> x0, waiting for transfers between devices: 75.1 us -> none  [on_device(): key_shard = lax.all_gather(key_proj, 'sp', axis=1, tiled=True)]
    ppermute x0 -> x3, waiting for transfers between devices: none -> 57.6 us  [on_device(): pieces = [lax.ppermute(pieces[0], 'sp', hops), *pieces]]
    all_gather x1, waiting for transfers between devices: 74.5 us -> 22.1 us  [on_device(): value_shard = lax.all_gather(value_proj, 'sp', axis=1, tiled=True)]
    unnamed x22 -> x35, local copies, waits for them, and re-layouts: 17 us -> 24.3 us
    ppermute x0 -> x3, starting transfers between devices: none -> 5.36 us  [on_device(): pieces = [lax.ppermute(pieces[0], 'sp', hops), *pieces]]
  transfers between devices with their start and end apart: 11 -> 13, of which waited for: 9 -> 9; matrix products, arithmetic and copies ran while one was open for 16% -> 21% of each run, Pallas kernels for 0% -> 0%
where the time goes in v1:
time: 427 us; the launch traced here: 426 us
  waiting for transfers between devices  298 us (70%)
  matrix products  46.3 us (11%)
  local copies, waits for them, and re-layouts  40.8 us (10%)
  other arithmetic  14.2 us (3%)
  between operations  13.6 us (3%)
  starting transfers between devices  9.66 us (2%)
    reduce_scatter x1, waiting for transfers between devices, on_device(): lax.psum_scatter((jnp.dot(pool_flat, out_pool_full, preferred_element_typ...  89.5 us
    all_gather x1, waiting for transfers between devices, on_device(): shard_rows = lax.all_gather(normed, 'tp', axis=1, tiled=True)  58.3 us
    ppermute x3, waiting for transfers between devices, on_device(): pieces = [lax.ppermute(pieces[0], 'sp', hops), *pieces]  57.6 us
    unnamed x35, local copies, waits for them, and re-layouts  24.3 us
    all_gather x1, waiting for transfers between devices, on_device(): value_shard = lax.all_gather(value_proj, 'sp', axis=1, tiled=True)  22.1 us
    all_gather x1, waiting for transfers between devices, on_device(): lax.all_gather(w_value, 'fs', axis=0, tiled=True)  19.9 us
    all_gather x1, waiting for transfers between devices, on_device(): lax.all_gather(w_key, 'fs', axis=0, tiled=True)  18.5 us
    all_gather x1, waiting for transfers between devices, on_device(): lax.all_gather(w_pool_in, 'fs', axis=0, tiled=True)  16.4 us
  transfers between devices with their start and end apart: 13, of which 9 were waited for; matrix products, arithmetic and copies ran while one was open for 21% of the time, Pallas kernels for 0%

profile of v1, /device:TPU:0, one launch (start us, length us, event | category | flops | bytes accessed | tf_op | source)
XLA Modules:
  0.0 425.9 jit_solution(2938594129094340023)
XLA Ops:
  6.5 0.7 all-gather.19.cloned.1.call-update
  7.3 2.1 fusion.15
  9.4 1.9 fusion.17
  12.7 1.0 copy.37
  14.4 19.9 %all-gather.19.cloned.1.call-done = bf16[2048,512]{1,0:T(8,128)(2,1)} async-done(((bf16[512,512]{1,0:T(8,128)(2,1)}), bf16[2048,512]{1,0:T(8,128)(2,1)}) %all-gather.19.cloned.1.call-update) | async-done | bytes 2097168 | tf_op jit(solution)/shard_map/all_gather | solution.py:83
  34.2 58.3 %all-gather.9.cloned.1.call-done = bf16[2,512,2048]{2,1,0:T(8,128)(2,1)} async-done(((bf16[2,256,2048]{2,1,0:T(8,128)(2,1)}), bf16[2,512,2048]{2,1,0:T(8,128)(2,1)}) %all-gather.9.cloned.1.call-update) | async-done | bytes 4194320 | tf_op jit(solution)/shard_map/all_gather | solution.py:89
  92.5 6.2 %fusion.35 = bf16[2,512,512]{2,1,0:T(8,128)(2,1)} fusion(bf16[2,512,2048]{2,1,0:T(8,128)(2,1)} %all-gather.9.cloned.1.call-done, bf16[2048,512]{1,0:T(8,128)(2,1)} %all-gather.19.cloned.1.call-done), kind=kOutput, calls=%fused_computation.44 | convolution fusion | flops 2148007936 | bytes 7340032 | tf_op jit(solution)/shard_map/dot_general | solution.py:97
  100.3 16.4 %all-gather.11.cloned.1.call-done = bf16[2048,512]{1,0:T(8,128)(2,1)} async-done(((bf16[512,512]{1,0:T(8,128)(2,1)}), bf16[2048,512]{1,0:T(8,128)(2,1)}) %all-gather.11.cloned.1.call-update) | async-done | bytes 2097168 | tf_op jit(solution)/shard_map/all_gather | solution.py:80
  116.7 5.2 %fusion.26 = bf16[2,512,512]{2,1,0:T(8,128)(2,1)S(1)} fusion(bf16[2,512,2048]{2,1,0:T(8,128)(2,1)} %all-gather.9.cloned.1.call-done, bf16[2048,512]{1,0:T(8,128)(2,1)} %all-gather.11.cloned.1.call-done), kind=kOutput, calls=%fused_computation.41 | convolution fusion | flops 2148007936 | bytes 7340032 | tf_op jit(solution)/shard_map/dot_general | solution.py:92
  122.2 18.5 %all-gather.15.cloned.1.call-done = bf16[2048,512]{1,0:T(8,128)(2,1)} async-done(((bf16[512,512]{1,0:T(8,128)(2,1)}), bf16[2048,512]{1,0:T(8,128)(2,1)}) %all-gather.15.cloned.1.call-update) | async-done | bytes 2097168 | tf_op jit(solution)/shard_map/all_gather | solution.py:82
  140.7 6.2 %fusion.29 = bf16[2,512,512]{2,1,0:T(8,128)(2,1)} fusion(bf16[2,512,2048]{2,1,0:T(8,128)(2,1)} %all-gather.9.cloned.1.call-done, bf16[2048,512]{1,0:T(8,128)(2,1)} %all-gather.15.cloned.1.call-done), kind=kOutput, calls=%fused_computation.42 | convolution fusion | flops 2148007936 | bytes 7340032 | tf_op jit(solution)/shard_map/dot_general | solution.py:96
  146.9 1.5 collective-permute-start.1
  148.4 4.0 collective-permute-start
  152.4 12.3 %all-gather.17.cloned.1.call-done = bf16[2048,512]{0,1:T(8,128)(2,1)} async-done(((bf16[512,512]{0,1:T(8,128)(2,1)}), bf16[2048,512]{0,1:T(8,128)(2,1)}) %all-gather.17.cloned.1.call-update) | async-done | bytes 2097168 | tf_op jit(solution)/shard_map/all_gather | solution.py:81
  164.7 6.2 %fusion.32 = bf16[2,512,512]{1,2,0:T(8,128)(2,1)} fusion(bf16[2,512,2048]{2,1,0:T(8,128)(2,1)} %all-gather.9.cloned.1.call-done, bf16[2048,512]{0,1:T(8,128)(2,1)} %all-gather.17.cloned.1.call-done), kind=kOutput, calls=%fused_computation.43 | convolution fusion | flops 2148007936 | bytes 7340032 | tf_op jit(solution)/shard_map/dot_general | solution.py:93
  170.9 2.3 copy.39
  173.2 0.7 fusion.71
  175.5 0.7 copy-done.2
  176.6 1.7 collective-permute-start.2
  178.3 2.2 fusion.67
  180.8 25.2 %collective-permute-done.2 = bf16[2,512,512]{2,1,0:T(8,128)(2,1)} collective-permute-done((bf16[2,512,512]{2,1,0:T(8,128)(2,1)}, bf16[2,512,512]{2,1,0:T(8,128)(2,1)}, u32[]{:S(2)}, u32[]{:S(2)}) %collective-permute-start.2) | collective-permute-done | bytes 1048608 | tf_op jit(solution)/shard_map/ppermute | solution.py:142
  206.1 2.2 collective-permute-start.3
  208.6 1.6 reshape.192
  210.2 2.3 copy.36
  213.2 1.6 copy.34
  214.8 1.5 multiply_convert_fusion.1
  216.4 7.3 %fusion.79 = f32[1024,2048]{1,0:T(8,128)} fusion(bf16[1024,512]{1,0:T(8,128)(2,1)S(1)} %bitcast.129, bf16[512,2048]{1,0:T(8,128)(2,1)} %all-gather.13.cloned.1.call-done), kind=kOutput, calls=%fused_computation.132 | convolution fusion | flops 2147483648 | bytes 11534336 | tf_op jit(solution)/shard_map/dot_general | solution.py:205
  223.7 32.4 %collective-permute-done.3 = bf16[2,512,512]{2,1,0:T(8,128)(2,1)S(1)} collective-permute-done((bf16[2,512,512]{2,1,0:T(8,128)(2,1)}, bf16[2,512,512]{2,1,0:T(8,128)(2,1)S(1)}, u32[]{:S(2)}, u32[]{:S(2)}) %collective-permute-start.3) | collective-permute-done | bytes 1048608 | tf_op jit(solution)/shard_map/ppermute | solution.py:142
  256.2 1.3 constant_dynamic-update-slice_fusion.6
  257.5 1.3 constant_dynamic-update-slice_fusion.5
  258.8 1.3 constant_dynamic-update-slice_fusion.4
  260.2 1.3 constant_dynamic-update-slice_fusion.2
  261.5 1.3 constant_dynamic-update-slice_fusion.1
  262.8 1.3 constant_dynamic-update-slice_fusion
  264.1 2.2 constant_dynamic-slice_fusion.3
  266.3 6.3 %copy.38 = bf16[2,2048,512]{1,2,0:T(8,128)(2,1)} copy(bf16[2,2048,512]{2,1,0:T(8,128)(2,1)} %constant_dynamic-slice_fusion.3) | data formatting | bytes 8388608
  272.6 22.1 %all-gather.21.cloned.1.call-done = bf16[2,2048,512]{2,1,0:T(8,128)(2,1)} async-done(((bf16[2,512,512]{2,1,0:T(8,128)(2,1)}), bf16[2,2048,512]{2,1,0:T(8,128)(2,1)}) %all-gather.21.cloned.1.call-update) | async-done | bytes 4194320 | tf_op jit(solution)/shard_map/all_gather | solution.py:146
  294.7 6.2 %copy.40 = bf16[2,2048,512]{1,2,0:T(8,128)(2,1)} copy(bf16[2,2048,512]{2,1,0:T(8,128)(2,1)} %all-gather.21.cloned.1.call-done) | data formatting | bytes 8388608
  301.2 1.0 copy-done.6
  302.2 17.2 %while.15 = (s32[]{:T(128)}, f32[2,512,4]{1,2,0:T(4,128)S(1)}, f32[2,512,4]{1,2,0:T(4,128)S(1)}, f32[2,512,4,128]{1,3,2,0:T(8,128)S(1)}, s32[4]{0:T(128)S(1)}, /...) while((s32[]{:T(128)}, f32[2,512,4]{1,2,0:T(4,128)S(1)}, ...), condition=%wide.region_6.7_spmd.clone, body=%wide.region_1.6_spmd.clone.sunk | while | flops 1114907648 | bytes 38154656 | solution.py:190
  303.5 12.0 %conditional.3 = ((f32[2,512,4]{1,2,0:T(4,128)S(1)}, f32[2,512,4]{1,2,0:T(4,128)S(1)}, f32[2,512,4,128]{1,3,2,0:T(8,128)S(1)})) conditional(s32[]{:T(128)} %convert_element_type.217, (f32[2,512,4]{1,2,0:T(4,128)S(1)}, f32[2,512,4]{1,2,0:T(4,128)S(1)}, f32[2,512,4,128]{1,3,2,0:T(8,128)S(1)}) %tuple.49, (s32[]{:T(128)}, s32[]{:T(128)}, s32[]{:T(128)}, ...), branch_computations={%region_2.2_spmd, %region_3.5_spmd} | conditional | flops 1114907648 | bytes 38152320 | solution.py:188
  304.4 1.7 constant_dynamic-slice_fusion
  306.1 2.6 fusion.6
  308.8 3.2 fusion.5
  312.0 3.5 bitcast_add_fusion.1
  320.0 1.5 copy.46
  321.5 8.4 %add_convert_fusion = bf16[1024,2048]{1,0:T(8,128)(2,1)} fusion(f32[1024,2048]{1,0:T(8,128)} %fusion.79, bf16[1024,512]{1,0:T(8,128)(2,1)S(1)} %bitcast.130, bf16[512,2048]{1,0:T(8,128)(2,1)} %all-gather.23.cloned.1.call-done), kind=kOutput, calls=%fused_computation.22 | convolution fusion | flops 2151677952 | bytes 15728640 | tf_op jit(solution)/shard_map/dot_general | solution.py:206
  329.9 89.5 %reduce-scatter.2.cloned.1.call-done = bf16[512,2048]{1,0:T(8,128)(2,1)} async-done(((bf16[1024,2048]{1,0:T(8,128)(2,1)}), bf16[512,2048]{1,0:T(8,128)(2,1)}) %reduce-scatter.2.cloned.1.call-update) | async-done | bytes 2097168 | tf_op jit(solution)/shard_map/reduce_scatter | solution.py:203
  (91 shorter events, 10.9 us)
Async XLA Ops:
  6.5 173.9 %copy-start = (bf16[8,128,128]{2,1,0:T(8,128)(2,1)S(1)}, bf16[8,128,128]{2,1,0:T(8,128)(2,1)}, u32[]{:S(2)}) copy-start(bf16[8,128,128]{2,1,0:T(8,128)(2,1)} %param.18) | copy-start | bytes 786436
  6.5 2.9 copy-start.4
  6.5 2.9 copy-start.9
  6.5 27.7 %all-gather.19.cloned.1.call-start = ((), (), s32[]{:S(2)}) async-start(), calls=%async_computation.6 | async-start | bytes 2621440 | tf_op jit(solution)/shard_map/all_gather | solution.py:83
  7.3 85.2 %all-gather.9.cloned.1.call-start = ((), (), s32[]{:S(2)}) async-start(), calls=%async_computation.1 | async-start | bytes 6291456 | tf_op jit(solution)/shard_map/all_gather | solution.py:89
  11.3 1.4 copy-start.7
  11.3 105.4 %all-gather.11.cloned.1.call-start = ((), (), s32[]{:S(2)}) async-start(), calls=%async_computation.2 | async-start | bytes 2621440 | tf_op jit(solution)/shard_map/all_gather | solution.py:80
  12.0 128.6 %all-gather.15.cloned.1.call-start = ((), (), s32[]{:S(2)}) async-start(), calls=%async_computation.4 | async-start | bytes 2621440 | tf_op jit(solution)/shard_map/all_gather | solution.py:82
  12.6 152.1 %all-gather.17.cloned.1.call-start = ((), (), s32[]{:S(2)}) async-start(), calls=%async_computation.5 | async-start | bytes 2621440 | tf_op jit(solution)/shard_map/all_gather | solution.py:81
  13.7 202.7 %all-gather.13.cloned.1.call-start = ((), (), s32[]{:S(2)}) async-start(), calls=%async_computation.3 | async-start | bytes 2621440 | tf_op jit(solution)/shard_map/all_gather | solution.py:84
  14.3 85.3 %copy-start.8 = (f32[2,4,2048]{2,1,0:T(4,128)S(1)}, f32[2,4,2048]{2,1,0:T(4,128)}, u32[]{:S(2)}) copy-start(f32[2,4,2048]{2,1,0:T(4,128)} %param.23) | copy-start | bytes 196612
  14.3 85.4 %copy-start.11 = (f32[1024]{0:T(1024)S(1)}, f32[1024]{0:T(1024)}, u32[]{:S(2)}) copy-start(f32[1024]{0:T(1024)} %param.19) | copy-start | bytes 12292
  14.3 280.4 %all-gather.21.cloned.1.call-start = ((), (), s32[]{:S(2)}) async-start(), calls=%async_computation.7 | async-start | bytes 5242880 | tf_op jit(solution)/shard_map/all_gather | solution.py:146
  98.7 222.7 %all-gather.23.cloned.1.call-start = ((), (), s32[]{:S(2)}) async-start(), calls=%async_computation.8 | async-start | bytes 2621440 | tf_op jit(solution)/shard_map/all_gather | solution.py:85
  99.5 319.9 %reduce-scatter.2.cloned.1.call-start = ((), (), s32[]{:S(2)}) async-start(), calls=%async_computation.9 | async-start | bytes 6291456 | tf_op jit(solution)/shard_map/reduce_scatter | solution.py:203
  146.9 29.7 %collective-permute-start.1 = (bf16[2,512,512]{2,1,0:T(8,128)(2,1)}, bf16[2,512,512]{2,1,0:T(8,128)(2,1)}, u32[]{:S(2)}, u32[]{:S(2)}) collective-permute-start(bf16[2,512,512]{2,1,0:T(8,128)(2,1)} %fusion.29), channel_id=1, source_target_pairs={{0,8},{8,16},{16,24},{24,0},{1,9},{9,17},{17,25},{25,1},{2,10},{10... | collective-permute-start | bytes 3145736 | tf_op jit(solution)/shard_map/ppermute | solution.py:142
  148.4 24.8 %collective-permute-start = (bf16[2,15,512]{2,1,0:T(8,128)(2,1)S(1)}, bf16[2,15,512]{2,1,0:T(8,128)(2,1)}, u32[]{:S(2)}, u32[]{:S(2)}) collective-permute-start(bf16[2,15,512]{2,1,0:T(8,128)(2,1)S(1)} %slice.84), channel_id=1, source_target_pairs={{0,8},{8,16},{16,24},{1,9},{9,17},{17,25},{2,10},{10,18},{18,26},{... | collective-permute-start | bytes 92168 | tf_op jit(solution)/shard_map/ppermute | solution.py:16
  175.3 1.0 copy-start.2
  176.3 2.0 copy-start.3
  176.3 2.0 slice-start
  176.6 29.5 %collective-permute-start.2 = (bf16[2,512,512]{2,1,0:T(8,128)(2,1)}, bf16[2,512,512]{2,1,0:T(8,128)(2,1)}, u32[]{:S(2)}, u32[]{:S(2)}) collective-permute-start(bf16[2,512,512]{2,1,0:T(8,128)(2,1)} %collective-permute-done.1), channel_id=1, source_target_pairs={{0,8},{8,16},{16,24},{24,0},{1,9},{9,17},{17,25},{25,1},{2,10},{10... | collective-permute-start | bytes 3145736 | tf_op jit(solution)/shard_map/ppermute | solution.py:142
  206.1 50.0 %collective-permute-start.3 = (bf16[2,512,512]{2,1,0:T(8,128)(2,1)}, bf16[2,512,512]{2,1,0:T(8,128)(2,1)S(1)}, u32[]{:S(2)}, u32[]{:S(2)}) collective-permute-start(bf16[2,512,512]{2,1,0:T(8,128)(2,1)} %collective-permute-done.2), channel_id=1, source_target_pairs={{0,8},{8,16},{16,24},{24,0},{1,9},{9,17},{17,25},{25,1},{2,10},{10... | collective-permute-start | bytes 3145736 | tf_op jit(solution)/shard_map/ppermute | solution.py:142
  212.5 2.3 copy-start.10
  213.2 1.6 copy-start.5
  300.9 1.3 copy-start.6
  329.9 89.5 %copy-start.1 = (bf16[8,128,128]{2,1,0:T(8,128)(2,1)S(1)}, bf16[8,128,128]{2,1,0:T(8,128)(2,1)}, u32[]{:S(2)}) copy-start(bf16[8,128,128]{2,1,0:T(8,128)(2,1)} %param.18) | copy-start | bytes 786436
Sparse Core Ops, SparseCore 0:
  8.9 25.2 all-gather.18
  35.8 56.7 all-gather.8
  94.1 22.5 all-gather.10
  118.1 22.5 all-gather.14
  142.1 22.5 all-gather.16
  166.1 22.5 all-gather.12
  190.3 104.3 all-gather.20
  296.2 20.4 all-gather.22
  330.1 89.2 reduce-scatter.1
